TPU v7x, 512 devices: a whole 4x4x16 slice. The times are simulated.
512 devices in a mesh: sp: 64 (over z, y), tp: 8 (over x, core).
Axes of the slice: x: 4, y: 4, z: 16, core: 2. Of those that a mesh axis runs over, the one named last changes fastest.
Arguments:
- resid: bfloat16 [16384, 2048], P(('sp', 'tp')), may hold values from -6 to 6
- queries: bfloat16 [16384, 1024], P('sp', 'tp'), may hold values from -6 to 6
- keys: bfloat16 [512, 16384], P('tp', 'sp'), may hold values from -6 to 6
- values: bfloat16 [512, 16384], P('tp', 'sp'), may hold values from -6 to 6
- log_gates: float32 [16, 16384], P('tp', 'sp'), may hold values from -1640 to 0, as said below
- q_gain: float32 [64], replicated, may hold values from 0.5 to 7
- k_gain: float32 [64], replicated, may hold values from 0.5 to 7
- w_out: bfloat16 [1024, 2048], P('tp'), may hold values from -0.1875 to 0.1875
- mlp_gain: bfloat16 [2048], replicated, may hold values from 0.099609375 to 1.8984375
- w_up: bfloat16 [2048, 8192], P('sp', 'tp'), may hold values from -0.125 to 0.125
- w_down: bfloat16 [8192, 2048], P('tp', 'sp'), may hold values from -0.0625 to 0.0625
Outputs:
- output: bfloat16 [16384, 2048], P(('sp', 'tp'))
Inputs may be any that keep to these rules, and one draw needn't show every extreme that they name: `log_gates`: each head's values never rise along positions.
All inputs are finite; a program needn't handle non-finite values.
Results may differ from a plain program's by a relative error of at most 0.018.
The roundings to bfloat16 on the way count: a program that leaves them out, or rounds other values in their place, can miss the bound.
Values may be sent and summed in bfloat16 or wider, within the bound.
No kernel may reach another device: no remote copies, remote signals or barrier semaphores. Data moves between devices by JAX's collectives and lax.ppermute only.
A program may use at most 64 MiB of HBM per device.

v0:
```python
import math
import jax
import jax.numpy as jnp
from jax import lax
from jax.sharding import PartitionSpec as P

EPS = 1e-06


def rows_first(arrays, axis, dims):
    turned = [jnp.moveaxis(a, dim, 0) for a, dim in zip(arrays, dims)]
    widths = [t[0].size for t in turned]
    both = jnp.concatenate([t.reshape(-1, w) for t, w in zip(turned, widths)], axis=1)
    result = lax.all_gather(both, axis, axis=0, tiled=True)
    parts = jnp.split(result, [sum(widths[:k]) for k in range(1, len(widths))], axis=1)
    return tuple(
        (
            jnp.moveaxis(b.reshape(-1, *t.shape[1:]), 0, dim)
            for b, t, dim in zip(parts, turned, dims)
        )
    )


def sent_to_all(value, axis):
    count = lax.axis_size(axis)
    return lax.all_to_all(
        jnp.broadcast_to(value[None], (count, *value.shape)), axis, 0, 0, tiled=True
    )


def joined_along(parts, dim):
    lengths = list(parts.shape[1:])
    lengths[dim] *= parts.shape[0]
    return jnp.moveaxis(parts, 0, dim).reshape(lengths)


def gather_directly(value, axis, dim):
    parts = sent_to_all(value, axis)
    return joined_along(parts, dim)


def in_one_piece(arrays, axis, dim, along):
    ends, at = ([], 0)
    for a in arrays[:-1]:
        at += a.shape[along]
        ends.append(at)
    both = jnp.concatenate(arrays, axis=along)
    return tuple(jnp.split(lax.all_gather(both, axis, axis=dim, tiled=True), ends, axis=along))


def cut_along(value, dim, count):
    before, after = (value.shape[:dim], value.shape[dim + 1 :])
    return jnp.moveaxis(value.reshape(*before, count, -1, *after), dim, 0)


def summed_on_arrival(value, axis, dim):
    count = lax.axis_size(axis)
    parts = lax.all_to_all(cut_along(value, dim, count), axis, 0, 0, tiled=True)
    return jnp.sum(parts.astype(jnp.float32), axis=0)


def rms_last(input_values, gain):
    scale = lax.rsqrt(jnp.mean(input_values * input_values, axis=-1, keepdims=True) + EPS)
    return input_values * scale * gain


def local(resid, queries, keys, values, log_gates, q_gain, k_gain, w_out, mlp_gain, w_up, w_down):
    up_whole, down_whole = rows_first((w_up, w_down), "sp", (0, 1))
    positions = queries.shape[0]
    head_size = q_gain.shape[0]
    query_count = log_gates.shape[0]
    key_total_count = keys.shape[0] // head_size
    group = query_count // key_total_count
    query_heads = queries.astype(jnp.float32).reshape(positions, query_count, head_size)
    qnorm = (rms_last(query_heads, q_gain) * head_size ** (-0.5)).astype(jnp.bfloat16)
    qnorm = jnp.transpose(qnorm.reshape(positions, key_total_count, group, head_size), (1, 2, 0, 3))
    key_heads = keys.astype(jnp.float32).reshape(key_total_count, head_size, positions)
    key_scale = lax.rsqrt(jnp.mean(key_heads * key_heads, axis=1, keepdims=True) + EPS)
    knorm = (key_heads * key_scale * k_gain[None, :, None]).astype(jnp.bfloat16)
    knorm = knorm.reshape(key_total_count * head_size, positions)
    gates_all = gather_directly(log_gates, "sp", 1)
    offset = lax.axis_index("sp") * positions
    query_pos = offset + jnp.arange(positions, dtype=jnp.int32)
    query_last = offset + positions - 1
    query_gates = log_gates.reshape(key_total_count, group, positions)
    start_state = (
        jnp.full((key_total_count, group, positions), -1e30, jnp.float32),
        jnp.zeros((key_total_count, group, positions), jnp.float32),
        jnp.zeros((key_total_count, group, positions, head_size), jnp.float32),
    )
    key_piece, value_piece = in_one_piece((knorm, values), "sp", 1, 0)
    length = key_piece.shape[1]
    block = math.gcd(length, 1024)
    key_blocks = key_piece.reshape(key_total_count, head_size, length)
    value_blocks = value_piece.reshape(key_total_count, head_size, length)

    def one_step(index, state):
        first = index * block

        def compute(inner):
            running_top, running_total, running_sum = inner
            key_now = lax.dynamic_slice_in_dim(key_blocks, index * block, block, 2)
            value_now = lax.dynamic_slice_in_dim(value_blocks, index * block, block, 2)
            gates_now = lax.dynamic_slice_in_dim(gates_all, first, block, 1).reshape(
                key_total_count, group, block
            )
            logits = jnp.einsum(
                "kgtd,kdn->kgtn", qnorm, key_now, preferred_element_type=jnp.float32
            )
            logits = logits + query_gates[..., None] - gates_now[:, :, None, :]
            key_pos = first + jnp.arange(block, dtype=jnp.int32)
            logits = jnp.where(key_pos[None, :] <= query_pos[:, None], logits, -jnp.inf)
            new_top = jnp.maximum(running_top, jnp.max(logits, axis=-1))
            rescale = jnp.exp(running_top - new_top)
            weights = jnp.exp(logits - new_top[..., None])
            new_total = running_total * rescale + jnp.sum(weights, axis=-1)
            product = jnp.einsum(
                "kgtn,kdn->kgtd",
                weights.astype(jnp.bfloat16),
                value_now,
                preferred_element_type=jnp.float32,
            )
            return (new_top, new_total, running_sum * rescale[..., None] + product)

        return lax.cond(first <= query_last, compute, lambda inner: inner, state)

    final_top, final_total, final_sum = lax.fori_loop(0, length // block, one_step, start_state)
    attn = final_sum / final_total[..., None]
    attn = (
        jnp.transpose(attn, (2, 0, 1, 3))
        .reshape(positions, query_count * head_size)
        .astype(jnp.bfloat16)
    )
    rows_now = attn
    proj = summed_on_arrival(
        jnp.dot(rows_now, w_out, preferred_element_type=jnp.float32).astype(jnp.bfloat16), "tp", 0
    )
    mixed = (resid.astype(jnp.float32) + proj).astype(jnp.bfloat16)
    normed = rms_last(mixed.astype(jnp.float32), mlp_gain.astype(jnp.float32)).astype(jnp.bfloat16)
    upward = jnp.dot(gather_directly(normed, "tp", 0), up_whole, preferred_element_type=jnp.float32)
    act = jnp.square(jax.nn.relu(upward)).astype(jnp.bfloat16)
    rows_now = act
    summed_down = summed_on_arrival(
        jnp.dot(rows_now, down_whole, preferred_element_type=jnp.float32).astype(jnp.bfloat16),
        "tp",
        0,
    )
    return (mixed.astype(jnp.float32) + summed_down).astype(jnp.bfloat16)


def solution(mesh):
    return jax.shard_map(
        local,
        mesh=mesh,
        in_specs=(
            P(("sp", "tp"), None),
            P("sp", "tp"),
            P("tp", "sp"),
            P("tp", "sp"),
            P("tp", "sp"),
            P(),
            P(),
            P("tp", None),
            P(),
            P("sp", "tp"),
            P("tp", "sp"),
        ),
        out_specs=P(("sp", "tp"), None),
        check_vma=False,
    )
```

profile of v0, /device:TPU:1, one launch (start us, length us, event | category | flops | bytes accessed | tf_op | source)
XLA Modules:
  0.0 348.9 jit_solution(38273085295830202)
XLA Ops:
  6.5 0.8 fusion.39
  7.4 0.8 fusion.41
  8.2 1.4 pad_maximum_fusion.1
  9.6 0.0 all-gather.3.cloned.1.call-update
  9.6 0.0 all-gather.5.cloned.1.call-start
  9.7 1.5 pad_maximum_fusion
  11.2 0.0 all-gather.5.cloned.1.call-update
  11.3 1.4 broadcast_in_dim.25
  12.6 19.3 %all-to-all-start = ((f32[64,2,256]{2,1,0:T(2,128)}), f32[64,2,256]{2,1,0:T(2,128)S(1)}, u32[]{:S(2)}, u32[]{:S(2)}) async-start(f32[64,2,256]{2,1,0:T(2,128)} %broadcast_in_dim.25), calls=%async_computation | async-start | bytes 262144 | tf_op jit(solution)/shard_map/all_to_all | solution.py:26
  31.9 0.9 copy.17
  32.9 0.7 fusion.42
  33.7 119.0 %all-gather.3.cloned.1.call-done = bf16[128,16384]{1,0:T(8,128)(2,1)} async-done(((bf16[128,256]{1,0:T(8,128)(2,1)}), bf16[128,16384]{1,0:T(8,128)(2,1)}) %all-gather.3.cloned.1.call-update) | async-done | bytes 4194320 | tf_op jit(solution)/shard_map/all_gather | solution.py:48
  152.6 3.9 %slice_bitcast_fusion = (bf16[1,64,16384]{2,1,0:T(8,128)(2,1)S(1)}, bf16[1,64,16384]{2,1,0:T(8,128)(2,1)}) fusion(bf16[128,16384]{1,0:T(8,128)(2,1)} %all-gather.3.cloned.1.call-done), kind=kLoop, calls=%fused_computation.30 | loop fusion | bytes 8388608 | tf_op jit(solution)/shard_map/reshape | solution.py:95
  156.6 3.4 while.18
  156.6 2.6 conditional.3
  156.7 0.2 broadcast_compare_fusion
  156.9 1.5 fusion.44
  158.4 0.5 fusion.5
  158.9 0.3 fusion.4
  160.1 1.5 convolution_convert_fusion
  161.6 14.5 %all-to-all-start.1 = ((bf16[8,32,2048]{2,1,0:T(8,128)(2,1)}), bf16[8,32,2048]{2,1,0:T(8,128)(2,1)S(1)}, u32[]{:S(2)}, u32[]{:S(2)}) async-start(bf16[8,32,2048]{2,1,0:T(8,128)(2,1)} %bitcast.21), calls=%async_computation.1 | async-start | bytes 2097152 | tf_op jit(solution)/shard_map/all_to_all | solution.py:58
  176.1 15.0 %all-to-all-done.1 = bf16[8,32,2048]{2,1,0:T(8,128)(2,1)S(1)} async-done(((bf16[8,32,2048]{2,1,0:T(8,128)(2,1)}), bf16[8,32,2048]{2,1,0:T(8,128)(2,1)S(1)}, u32[]{:S(2)}, u32[]{:S(2)}) %all-to-all-start.1) | async-done | bytes 1048608 | tf_op jit(solution)/shard_map/all_to_all | solution.py:58
  191.1 0.1 convert_reduce_fusion.1
  191.2 0.2 fusion.35
  191.4 0.1 fusion.37
  191.5 0.1 broadcast_in_dim.26
  191.6 18.3 %all_to_all.20 = bf16[8,32,2048]{2,1,0:T(8,128)(2,1)S(1)} all-to-all(bf16[8,32,2048]{2,1,0:T(8,128)(2,1)S(1)} %broadcast_in_dim.26), channel_id=1, replica_groups=mesh['sp'=64,'tp'=8] {'tp'}, dimensions={0} | all-to-all | bytes 2097152 | tf_op jit(solution)/shard_map/all_to_all | solution.py:26
  209.9 98.1 %all-gather.5.cloned.1.call-done = bf16[2048,2048]{1,0:T(8,128)(2,1)} async-done(((bf16[32,2048]{1,0:T(8,128)(2,1)}), bf16[2048,2048]{1,0:T(8,128)(2,1)}) %all-gather.5.cloned.1.call-update) | async-done | bytes 8388624 | tf_op jit(solution)/shard_map/all_gather | solution.py:14
  308.0 5.8 %fusion.20 = bf16[256,2048]{1,0:T(8,128)(2,1)S(1)} fusion(bf16[2048,2048]{1,0:T(8,128)(2,1)} %all-gather.5.cloned.1.call-done, bf16[256,2048]{1,0:T(8,128)(2,1)S(1)} %bitcast.57), kind=kOutput, calls=%fused_computation.29 | convolution fusion | flops 2148794368 | bytes 10485760 | tf_op jit(solution)/shard_map/dot_general | solution.py:144
  313.9 27.4 %all_to_all.21 = bf16[8,32,2048]{2,1,0:T(8,128)(2,1)S(1)} all-to-all(bf16[8,32,2048]{2,1,0:T(8,128)(2,1)S(1)} %bitcast.58), channel_id=1, replica_groups=mesh['sp'=64,'tp'=8] {'tp'}, dimensions={0} | all-to-all | bytes 2097152 | tf_op jit(solution)/shard_map/all_to_all | solution.py:58
  341.3 0.1 convert_reduce_fusion
  341.4 0.7 fusion.38
  (56 shorter events, 0.4 us)
Async XLA Ops:
  6.5 153.5 %copy-start = (bf16[128,2048]{1,0:T(8,128)(2,1)S(1)}, bf16[128,2048]{1,0:T(8,128)(2,1)}, u32[]{:S(2)}) copy-start(bf16[128,2048]{1,0:T(8,128)(2,1)} %param.22) | copy-start | bytes 1572868
  6.5 146.1 %all-gather.3.cloned.1.call-start = ((), (), s32[]{:S(2)}) async-start(), calls=%async_computation.4 | async-start | bytes 4259840 | tf_op jit(solution)/shard_map/all_gather | solution.py:48
  9.6 298.4 %all-gather.5.cloned.1.call-start = ((), (), s32[]{:S(2)}) async-start(), calls=%async_computation.5 | async-start | bytes 8519680 | tf_op jit(solution)/shard_map/all_gather | solution.py:14
  12.6 143.9 %all-to-all-start = ((f32[64,2,256]{2,1,0:T(2,128)}), f32[64,2,256]{2,1,0:T(2,128)S(1)}, u32[]{:S(2)}, u32[]{:S(2)}) async-start(f32[64,2,256]{2,1,0:T(2,128)} %broadcast_in_dim.25), calls=%async_computation | async-start | bytes 262144 | tf_op jit(solution)/shard_map/all_to_all | solution.py:26
  33.6 122.9 %copy-start.3 = (f32[2,256]{1,0:T(2,128)S(1)}, f32[2,256]{1,0:T(2,128)}, u32[]{:S(2)}) copy-start(f32[2,256]{1,0:T(2,128)} %param.19) | copy-start | bytes 6148
  160.0 16.1 %copy-start.2 = (bf16[2048]{0:T(1024)(128)(2,1)S(1)}, bf16[2048]{0:T(1024)(128)(2,1)}, u32[]{:S(2)}) copy-start(bf16[2048]{0:T(1024)(128)(2,1)} %param.23) | copy-start | bytes 12292
  161.6 29.6 %copy-start.1 = (bf16[32,2048]{1,0:T(8,128)(2,1)S(1)}, bf16[32,2048]{1,0:T(8,128)(2,1)}, u32[]{:S(2)}) copy-start(bf16[32,2048]{1,0:T(8,128)(2,1)} %param.15) | copy-start | bytes 393220
  161.6 29.5 %all-to-all-start.1 = ((bf16[8,32,2048]{2,1,0:T(8,128)(2,1)}), bf16[8,32,2048]{2,1,0:T(8,128)(2,1)S(1)}, u32[]{:S(2)}, u32[]{:S(2)}) async-start(bf16[8,32,2048]{2,1,0:T(8,128)(2,1)} %bitcast.21), calls=%async_computation.1 | async-start | bytes 2097152 | tf_op jit(solution)/shard_map/all_to_all | solution.py:58
Sparse Core Ops, SparseCore 0:
  10.2 142.3 all-gather.2
  155.6 152.4 all-gather.4
where the time goes:
time: 350 us; the launch traced here: 349 us
  waiting for transfers between devices  232 us (66%)
  blocking collectives  45.7 us (13%)
  starting transfers between devices  33.8 us (10%)
  between operations  13.6 us (4%)
  matrix products  9.29 us (3%)
  other arithmetic  7.18 us (2%)
  local copies, waits for them, and re-layouts  6.37 us (2%)
    all_gather x1, waiting for transfers between devices, in_one_piece(): lax.all_gather(both, axis, axis=dim, tiled=True)  119 us
    all_gather x1, waiting for transfers between devices, rows_first(): result = lax.all_gather(both, axis, axis=0, tiled=True)  98.1 us
    all_to_all x1, blocking collectives, summed_on_arrival(): parts = lax.all_to_all(cut_along(value, dim, count), axis, 0, 0, tiled=True)  27.4 us
    all_to_all x1, starting transfers between devices, sent_to_all(): lax.all_to_all(jnp.broadcast_to(value[None], (count, *value.shape)), axis...  19.3 us
    all_to_all x1, blocking collectives, sent_to_all(): lax.all_to_all(jnp.broadcast_to(value[None], (count, *value.shape)), axis...  18.3 us
    all_to_all x1, waiting for transfers between devices, summed_on_arrival(): parts = lax.all_to_all(cut_along(value, dim, count), axis, 0, 0, tiled=True)  15 us
    all_to_all x1, starting transfers between devices, summed_on_arrival(): parts = lax.all_to_all(cut_along(value, dim, count), axis, 0, 0, tiled=True)  14.5 us
  transfers between devices with their start and end apart: 4, of which 3 were waited for; matrix products, arithmetic and copies ran while one was open for 4% of the time, Pallas kernels for 0%

commit v1 on v0

--- a/solution.py
+++ b/solution.py
@@ -7,11 +7,16 @@
 EPS = 1e-06
 
 
+def _render_things(view, mesh_ax):
+    answer = jnp.stack([view] * lax.axis_size(mesh_ax))
+    return jnp.concatenate(lax.all_to_all(answer, mesh_ax, 0, 0), axis=0)
+
+
 def rows_first(arrays, axis, dims):
     turned = [jnp.moveaxis(a, dim, 0) for a, dim in zip(arrays, dims)]
     widths = [t[0].size for t in turned]
     both = jnp.concatenate([t.reshape(-1, w) for t, w in zip(turned, widths)], axis=1)
-    result = lax.all_gather(both, axis, axis=0, tiled=True)
+    result = _render_things(both, axis)
     parts = jnp.split(result, [sum(widths[:k]) for k in range(1, len(widths))], axis=1)
     return tuple(
         (

time: 350 us -> 660 us (1.89)
  blocking collectives: 45.7 us -> 432 us
  waiting for transfers between devices: 232 us -> 150 us
    all_to_all x1, blocking collectives: 18.3 us -> 409 us  [_render_things(): return jnp.concatenate(lax.all_to_all(answer, mesh_ax, 0, 0), axis=0)]
    all_gather x1 -> x0, waiting for transfers between devices: 98.1 us -> none  [rows_first(): result = lax.all_gather(both, axis, axis=0, tiled=True)]
    all_to_all x1 -> x2, waiting for transfers between devices: 0.01 us -> 15 us  [sent_to_all(): lax.all_to_all(jnp.broadcast_to(value[None], (count, *value.shape)), axis...]
    all_to_all x1 -> x2, starting transfers between devices: 19.3 us -> 23.7 us  [sent_to_all(): lax.all_to_all(jnp.broadcast_to(value[None], (count, *value.shape)), axis...]
  transfers between devices with their start and end apart: 4 -> 4, of which waited for: 3 -> 3; matrix products, arithmetic and copies ran while one was open for 4% -> 1% of each run, Pallas kernels for 0% -> 0%
where the time goes in v1:
time: 660 us; the launch traced here: 659 us
  blocking collectives  432 us (65%)
  waiting for transfers between devices  150 us (23%)
  starting transfers between devices  38.2 us (6%)
  between operations  13.6 us (2%)
  matrix products  9.21 us (1%)
  local copies, waits for them, and re-layouts  8.41 us (1%)
    all_to_all x1, blocking collectives, _render_things(): return jnp.concatenate(lax.all_to_all(answer, mesh_ax, 0, 0), axis=0)  409 us
    all_gather x1, waiting for transfers between devices, in_one_piece(): lax.all_gather(both, axis, axis=dim, tiled=True)  120 us
    all_to_all x1, blocking collectives, summed_on_arrival(): parts = lax.all_to_all(cut_along(value, dim, count), axis, 0, 0, tiled=True)  23.8 us
    all_to_all x2, starting transfers between devices, sent_to_all(): lax.all_to_all(jnp.broadcast_to(value[None], (count, *value.shape)), axis...  23.7 us
    all_to_all x2, waiting for transfers between devices, sent_to_all(): lax.all_to_all(jnp.broadcast_to(value[None], (count, *value.shape)), axis...  15 us
    all_to_all x1, waiting for transfers between devices, summed_on_arrival(): parts = lax.all_to_all(cut_along(value, dim, count), axis, 0, 0, tiled=True)  15 us
    all_to_all x1, starting transfers between devices, summed_on_arrival(): parts = lax.all_to_all(cut_along(value, dim, count), axis, 0, 0, tiled=True)  14.5 us
  transfers between devices with their start and end apart: 4, of which 3 were waited for; matrix products, arithmetic and copies ran while one was open for 1% of the time, Pallas kernels for 0%

profile of v1, /device:TPU:1, one launch (start us, length us, event | category | flops | bytes accessed | tf_op | source)
XLA Modules:
  0.0 658.8 jit_solution(7782676902349739408)
XLA Ops:
  6.5 0.8 fusion.39
  7.4 0.8 fusion.41
  8.2 1.4 pad_maximum_fusion.1
  9.6 0.0 all-gather.2.cloned.1.call-update
  9.6 1.4 broadcast_in_dim.25
  11.0 19.3 %all-to-all-start = ((f32[64,2,256]{2,1,0:T(2,128)}), f32[64,2,256]{2,1,0:T(2,128)S(1)}, u32[]{:S(2)}, u32[]{:S(2)}) async-start(f32[64,2,256]{2,1,0:T(2,128)} %broadcast_in_dim.25), calls=%async_computation | async-start | bytes 262144 | tf_op jit(solution)/shard_map/all_to_all | solution.py:31
  30.3 0.9 copy.17
  31.3 0.7 fusion.42
  32.0 0.0 copy-start.5
  32.1 120.4 %all-gather.2.cloned.1.call-done = bf16[128,16384]{1,0:T(8,128)(2,1)} async-done(((bf16[128,256]{1,0:T(8,128)(2,1)}), bf16[128,16384]{1,0:T(8,128)(2,1)}) %all-gather.2.cloned.1.call-update) | async-done | bytes 4194320 | tf_op jit(solution)/shard_map/all_gather | solution.py:53
  152.5 3.9 slice_bitcast_fusion
  156.4 3.5 while.18
  156.4 2.6 conditional.3
  156.5 0.2 broadcast_compare_fusion
  156.7 1.5 fusion.44
  158.2 0.3 fusion.4
  158.5 0.5 fusion.5
  159.9 1.4 convolution_convert_fusion
  161.3 14.5 %all-to-all-start.1 = ((bf16[8,32,2048]{2,1,0:T(8,128)(2,1)}), bf16[8,32,2048]{2,1,0:T(8,128)(2,1)S(1)}, u32[]{:S(2)}, u32[]{:S(2)}) async-start(bf16[8,32,2048]{2,1,0:T(8,128)(2,1)} %bitcast.21), calls=%async_computation.1 | async-start | bytes 2097152 | tf_op jit(solution)/shard_map/all_to_all | solution.py:63
  175.9 15.0 %all-to-all-done.1 = bf16[8,32,2048]{2,1,0:T(8,128)(2,1)S(1)} async-done(((bf16[8,32,2048]{2,1,0:T(8,128)(2,1)}), bf16[8,32,2048]{2,1,0:T(8,128)(2,1)S(1)}, u32[]{:S(2)}, u32[]{:S(2)}) %all-to-all-start.1) | async-done | bytes 1048608 | tf_op jit(solution)/shard_map/all_to_all | solution.py:63
  190.9 0.1 convert_reduce_fusion.1
  191.0 0.2 fusion.35
  191.2 0.1 fusion.37
  191.3 1.1 broadcast_in_dim.26
  192.4 4.4 all-to-all-start.2
  196.9 15.0 %all-to-all-done.2 = bf16[8,32,2048]{2,1,0:T(8,128)(2,1)S(1)} async-done(((bf16[8,32,2048]{2,1,0:T(8,128)(2,1)}), bf16[8,32,2048]{2,1,0:T(8,128)(2,1)S(1)}, u32[]{:S(2)}, u32[]{:S(2)}) %all-to-all-start.2) | async-done | bytes 1048608 | tf_op jit(solution)/shard_map/all_to_all | solution.py:31
  211.8 1.1 stack.2
  212.9 408.6 %all_to_all.25 = bf16[64,32,2048]{2,1,0:T(8,128)(2,1)} all-to-all(bf16[64,32,2048]{2,1,0:T(8,128)(2,1)S(1)} %stack.2), channel_id=1, replica_groups=mesh['sp'=64,'tp'=8] {'sp'}, dimensions={0} | all-to-all | bytes 16777216 | tf_op jit(solution)/shard_map/all_to_all | solution.py:12
  621.5 5.8 fusion.20
  627.3 23.8 %all_to_all.26 = bf16[8,32,2048]{2,1,0:T(8,128)(2,1)S(1)} all-to-all(bf16[8,32,2048]{2,1,0:T(8,128)(2,1)S(1)} %bitcast.60), channel_id=1, replica_groups=mesh['sp'=64,'tp'=8] {'tp'}, dimensions={0} | all-to-all | bytes 2097152 | tf_op jit(solution)/shard_map/all_to_all | solution.py:63
  651.1 0.1 convert_reduce_fusion
  651.3 0.7 fusion.38
  (60 shorter events, 0.4 us)
Async XLA Ops:
  6.5 153.4 %copy-start = (bf16[128,2048]{1,0:T(8,128)(2,1)S(1)}, bf16[128,2048]{1,0:T(8,128)(2,1)}, u32[]{:S(2)}) copy-start(bf16[128,2048]{1,0:T(8,128)(2,1)} %param.22) | copy-start | bytes 1572868
  6.5 145.9 %all-gather.2.cloned.1.call-start = ((), (), s32[]{:S(2)}) async-start(), calls=%async_computation.5 | async-start | bytes 4259840 | tf_op jit(solution)/shard_map/all_gather | solution.py:53
  11.0 145.3 %all-to-all-start = ((f32[64,2,256]{2,1,0:T(2,128)}), f32[64,2,256]{2,1,0:T(2,128)S(1)}, u32[]{:S(2)}, u32[]{:S(2)}) async-start(f32[64,2,256]{2,1,0:T(2,128)} %broadcast_in_dim.25), calls=%async_computation | async-start | bytes 262144 | tf_op jit(solution)/shard_map/all_to_all | solution.py:31
  32.0 124.3 %copy-start.5 = (f32[2,256]{1,0:T(2,128)S(1)}, f32[2,256]{1,0:T(2,128)}, u32[]{:S(2)}) copy-start(f32[2,256]{1,0:T(2,128)} %param.19) | copy-start | bytes 6148
  159.9 16.0 %copy-start.4 = (bf16[2048]{0:T(1024)(128)(2,1)S(1)}, bf16[2048]{0:T(1024)(128)(2,1)}, u32[]{:S(2)}) copy-start(bf16[2048]{0:T(1024)(128)(2,1)} %param.23) | copy-start | bytes 12292
  161.3 29.7 %copy-start.1 = (bf16[32,2048]{1,0:T(8,128)(2,1)S(1)}, bf16[32,2048]{1,0:T(8,128)(2,1)}, u32[]{:S(2)}) copy-start(bf16[32,2048]{1,0:T(8,128)(2,1)} %param.15) | copy-start | bytes 393220
  161.3 29.5 %all-to-all-start.1 = ((bf16[8,32,2048]{2,1,0:T(8,128)(2,1)}), bf16[8,32,2048]{2,1,0:T(8,128)(2,1)S(1)}, u32[]{:S(2)}, u32[]{:S(2)}) async-start(bf16[8,32,2048]{2,1,0:T(8,128)(2,1)} %bitcast.21), calls=%async_computation.1 | async-start | bytes 2097152 | tf_op jit(solution)/shard_map/all_to_all | solution.py:63
  191.0 5.8 copy-start.2
  191.0 5.8 copy-start.3
  192.4 19.4 %all-to-all-start.2 = ((bf16[8,32,2048]{2,1,0:T(8,128)(2,1)}), bf16[8,32,2048]{2,1,0:T(8,128)(2,1)S(1)}, u32[]{:S(2)}, u32[]{:S(2)}) async-start(bf16[8,32,2048]{2,1,0:T(8,128)(2,1)} %broadcast_in_dim.26), calls=%async_computation.2 | async-start | bytes 2097152 | tf_op jit(solution)/shard_map/all_to_all | solution.py:31
Sparse Core Ops, SparseCore 0:
  10.2 142.1 all-gather.1
